TPU v7x, 32 devices: a whole 2x2x4 slice. The times are simulated.
32 devices in a mesh: sp: 4 (over y, x), dp: 8 (over z, core).
Axes of the slice: x: 2, y: 2, z: 4, core: 2. Of those that a mesh axis runs over, the one named last changes fastest.
Arguments:
- tokens: bfloat16 [8, 768, 4096], P('dp', 'sp'), may hold values from -30 to 30
- query_weight: bfloat16 [4096, 512], P('dp', 'sp'), may hold values from -0.09375 to 0.09375
- key_weight: bfloat16 [4096, 512], P('dp', 'sp'), may hold values from -0.09375 to 0.09375
- value_weight: bfloat16 [4096, 512], P('dp', 'sp'), may hold values from -0.09375 to 0.09375
- cum_gate: float32 [8, 4, 768], P('dp', 'sp'), may hold values from -3072 to 0, as said below
Outputs:
- attended: bfloat16 [8, 768, 512], P('dp', 'sp')
Inputs may be any that keep to these rules, and one draw needn't show every extreme that they name: `cum_gate`: never rising along positions; the first position holds one step's log gate.
All inputs are finite; a program needn't handle non-finite values.
Results may differ from a plain program's by a relative error of at most 0.0076.
The roundings to bfloat16 on the way count: a program that leaves them out, or rounds other values in their place, can miss the bound.
Values may be sent and summed in bfloat16 or wider, within the bound.
A program may use at most 128 MiB of HBM per device.

v0:
```python
import functools
import math

import jax
import jax.numpy as jnp
from jax import lax
from jax.experimental import pallas as pl
from jax.experimental.pallas import tpu as pltpu
from jax.sharding import PartitionSpec as P

MESH = pl.DeviceIdType.MESH


def kernel(
    nx, ny, nz, cores, split, early, cuts, kept,
    tok_hbm, wq_hbm, wk_hbm, wv_hbm, gate_hbm, out_ref,
    xbuf, wbuf, acc, qkv, qout, gate_ref, gcol, attn, bias,
    lsem, tsem, gsem, xsend, xrecv, ownrecv, farrecv, precv, zsend, sideq, sidesem, psem,
    qsend, qrecv, osend, orecv,
):
    tok, depth = tok_hbm.shape
    rows, head = wq_hbm.shape
    chunk = cores * rows
    group = nx * tok
    length = ny * group
    s, d = lax.axis_index("sp"), lax.axis_index("dp")
    y, x = s // nx, s % nx
    z, c = d // cores, d % cores
    others = [(y + k) % ny for k in range(1, ny)]
    early_rows = pl.ds(0, early)
    late_rows = pl.ds(early, rows - early)
    whole = pl.ds(0, rows)
    parts = (pl.ds(0, split), pl.ds(split, tok - split))

    def columns(zb):
        return pl.ds(pl.multiple_of(zb * chunk, chunk), chunk)

    low = jnp.minimum(z, nz - 1 - z)

    def nearest(k):
        if k == 0:
            return z
        near = z - (k + 1) // 2 if k % 2 else z + k // 2
        far = jnp.where(z < nz - 1 - z, z + k - low, z - k + low)
        return jnp.where(k <= 2 * low, near, far)

    loads = [
        pltpu.make_async_copy(ref, wbuf.at[y, z, c, :, pl.ds(i * head, head)], lsem)
        for i, ref in enumerate((wq_hbm, wk_hbm, wv_hbm))
    ]
    own_load = pltpu.make_async_copy(tok_hbm, xbuf.at[x], tsem)
    for load in loads:
        load.start()
    own_load.start()
    gate_load = pltpu.make_async_copy(gate_hbm, gate_ref, gsem)
    gate_load.start()

    barrier = pltpu.get_barrier_semaphore()
    peers = [y * nx + (x + j) % nx for j in range(1, nx)]
    peers += [((y + k) % ny) * nx + x for k in range(1, ny)]
    for peer in peers:
        pl.semaphore_signal(barrier, inc=1, device_id={"sp": peer}, device_id_type=MESH)
    above = {"dp": jnp.minimum(z + 1, nz - 1) * cores + c}
    below = {"dp": jnp.maximum(z - 1, 0) * cores + c}
    beside = {"dp": z * cores + 1 - c}

    @pl.when(z < nz - 1)
    def _():
        pl.semaphore_signal(barrier, inc=1, device_id=above, device_id_type=MESH)

    @pl.when(z > 0)
    def _():
        pl.semaphore_signal(barrier, inc=1, device_id=below, device_id_type=MESH)

    if cores > 1:
        pl.semaphore_signal(barrier, inc=1, device_id=beside, device_id_type=MESH)
    inner = (z > 0) & (z < nz - 1)
    levels = jnp.where(inner, 2, 1) if nz > 1 else 0
    pl.semaphore_wait(barrier, len(peers) + cores - 1 + levels)

    def aside(k):
        return {"sp": ((y + k) % ny) * nx + x}

    def send_tokens(j, zb, g):
        return pltpu.make_async_remote_copy(
            src_ref=tok_hbm.at[parts[g], columns(zb)],
            dst_ref=xbuf.at[x, parts[g], columns(zb)],
            send_sem=xsend.at[j - 1], recv_sem=xrecv.at[j - 1, zb, g],
            device_id={"sp": y * nx + (x + j) % nx}, device_id_type=MESH,
        )

    def tokens_here(zb, g):
        for j in range(1, nx):
            i = (x - j + nx) % nx
            pltpu.make_async_remote_copy(
                src_ref=tok_hbm.at[parts[g], columns(zb)],
                dst_ref=xbuf.at[i, parts[g], columns(zb)],
                send_sem=xsend.at[j - 1], recv_sem=xrecv.at[j - 1, zb, g],
                device_id={"sp": y * nx + i}, device_id_type=MESH,
            ).wait_recv()

    def piece(which, p):
        size = early // cuts[1] if which else (rows - early) // cuts[0]
        return pl.ds(pl.multiple_of((0 if which else early) + p * size, 8), size)

    def mark(which, p):
        return p if which else cuts[1] + p

    def copy_block(h, zb, core, part, send_sem, recv_sem, device):
        ref = wbuf.at[h, zb, core, part]
        return pltpu.make_async_remote_copy(
            src_ref=ref, dst_ref=ref, send_sem=send_sem, recv_sem=recv_sem,
            device_id=device, device_id_type=MESH,
        )

    def landing(h, zb, p, place):
        for k in range(1, ny):
            if h is others[k - 1]:
                return farrecv.at[k - 1, zb, p]
        return ownrecv.at[place, p]

    def up(h, zb, part, p):
        return copy_block(h, zb, c, part, zsend.at[h, zb], landing(h, zb, p, zb), above)

    def down(h, zb, part, p):
        way = jnp.where(zb == z, nz, zb)
        return copy_block(
            h, zb, c, part, zsend.at[h, way], landing(h, zb, p, jnp.maximum(zb - 1, 0)), below
        )

    def side_early(k, p):
        return copy_block(
            y, z, c, piece(1, p), sideq.at[k - 1], farrecv.at[ny - k - 1, z, p], aside(k)
        )

    def side(k, zb, part):
        return copy_block(
            y, zb, c, part, sidesem.at[k - 1], farrecv.at[ny - k - 1, zb, cuts[1]], aside(k)
        )

    def pair(h, zb, part, core):
        return copy_block(h, zb, core, part, psem, precv.at[h, zb], beside)

    def arrived(h, zb, part, p):
        place = jnp.where(zb < z, zb, jnp.maximum(zb - 1, 0))
        copy_block(h, zb, c, part, lsem, landing(h, zb, p, place), aside(1)).wait_recv()

    def share(h, zb, which):
        if cores > 1:
            pair(h, zb, early_rows if which else late_rows, c).start()

    def shared(h, zb):
        if cores > 1:
            pair(h, zb, whole, 1 - c).wait_recv()

    def rise(h, zb, which, p):
        pl.when(z < nz - 1)(lambda: up(h, zb, piece(which, p), mark(which, p)).start())

    def sink(h, zb, which, p):
        pl.when(z > 0)(lambda: down(h, zb, piece(which, p), mark(which, p)).start())

    def both_ways(h, zb, which, p):
        rise(h, zb, which, p)
        sink(h, zb, which, p)

    def each(t, act):
        pl.when(z - t >= 0)(lambda: act(z - t, rise))
        pl.when(z + t < nz)(lambda: act(z + t, sink))

    def loop(which, act):
        def step(p, carry):
            act(p)
            return carry

        lax.fori_loop(0, cuts[which], step, 0)

    def relay_own(t):
        def take(p):
            def one(zb, onward):
                arrived(y, zb, piece(0, p), mark(0, p))
                onward(y, zb, 0, p)
                for k in range(1, ny):
                    side(k, zb, piece(0, p)).start()

            each(t, one)

        loop(0, take)
        each(t, lambda zb, onward: share(y, zb, 0))

    def relay_last(t, rising):
        zb, onward = (z - t, rise) if rising else (z + t, sink)

        @pl.when(zb >= 0 if rising else zb < nz)
        def _():
            def take(p):
                arrived(y, zb, piece(1, p), p)
                onward(y, zb, 1, p)

            loop(1, take)
            share(y, zb, 1)

    def finish_way(rising, steps):
        loop(1, lambda p: (rise if rising else sink)(y, z, 1, p))
        for t in range(1, steps + 1):
            relay_last(t, rising)

    def relay_other(t):
        def take(p):
            for h in others:
                if t == 0:
                    arrived(h, z, piece(1, p), p)
                    both_ways(h, z, 1, p)
                    continue

                def one(zb, onward, h=h):
                    arrived(h, zb, piece(1, p), p)
                    onward(h, zb, 1, p)

                each(t, one)

        loop(1, take)
        for h in others:
            if t == 0:
                share(h, z, 1)
            else:
                each(t, lambda zb, onward, h=h: share(h, zb, 1))

    for k in range(nz):
        for j in range(1, nx):
            send_tokens(j, nearest(k), 0).start()
    for k in range(nz):
        for j in range(1, nx):
            send_tokens(j, nearest(k), 1).start()
    pltpu.make_async_copy(wbuf.at[y, z, c], wbuf.at[y, z, c], lsem).wait()
    loop(1, lambda p: [side_early(k, p).start() for k in range(1, ny)] and None)
    loop(0, lambda p: both_ways(y, z, 0, p))
    for k in range(1, ny):
        side(k, z, late_rows).start()
    share(y, z, 0)
    share(y, z, 1)

    gate_load.wait()
    for start in range(0, length, 128):
        row = gate_ref[:, start : start + 128]
        gcol[start : start + 128, :] = jnp.broadcast_to(row, (128, 128)).T
    acc[...] = jnp.zeros_like(acc)
    log2e = math.log2(math.e)

    def bias_of(at, size, extent):
        gap = gcol[pl.ds(at, size), :1] - gate_ref[:, :extent]
        rows_at = at + lax.broadcasted_iota(jnp.int32, gap.shape, 0)
        cols_at = lax.broadcasted_iota(jnp.int32, gap.shape, 1)
        return jnp.where(cols_at <= rows_at, gap * log2e, -1e30)

    if kept:
        for r in range(ny):
            for i in range(nx):
                at, extent = (r * nx + i) * tok, (r + 1) * group
                bias[at : at + tok, :extent] = bias_of(at, tok, extent)
    own_load.wait()

    def add(h, zb, i, part):
        weights = wbuf[h, zb].reshape(chunk, 3 * head)
        acc[h, i, part, :] += jnp.dot(
            xbuf[i, part, columns(zb)], weights, preferred_element_type=jnp.float32
        )

    everything = pl.ds(0, tok)

    def own_rows(i, g):
        at = y * group + i * tok + (split if g else 0)
        return pl.ds(pl.multiple_of(at, 16), parts[g].size)

    def send_qkv(k, i, g):
        return pltpu.make_async_remote_copy(
            src_ref=qout.at[k - 1, i, parts[g]], dst_ref=qkv.at[own_rows(i, g)],
            send_sem=qsend.at[k - 1], recv_sem=qrecv.at[ny - k - 1],
            device_id=aside(k), device_id_type=MESH,
        )

    def swap(i, g):
        for k in range(1, ny):
            qout[k - 1, i, parts[g], :] = acc[others[k - 1], i, parts[g], :].astype(jnp.bfloat16)
            send_qkv(k, i, g).start()

    def take_side(k):
        for h in others:
            arrived(h, nearest(k), late_rows, cuts[1])
            share(h, nearest(k), 0)

    def add_others(k):
        zb = nearest(k)
        for h in others:
            shared(h, zb)
            add(h, zb, x, everything)
        if k == nz - 1:
            for g in range(2):
                swap(x, g)
        tokens_here(zb, 0)
        for h in others:
            for j in range(1, nx):
                add(h, zb, (x + j) % nx, parts[0])

    def add_last_rows(k):
        zb = nearest(k)
        tokens_here(zb, 1)
        for h in others:
            for j in range(1, nx):
                add(h, zb, (x + j) % nx, parts[1])

    def take_last(k):
        zb = nearest(k)

        @pl.when(jnp.logical_not(inner))
        def _():
            loop(1, lambda p: arrived(y, zb, piece(1, p), p))
            share(y, zb, 1)

    def add_own(k):
        zb = nearest(k)
        shared(y, zb)
        for i in range(nx):
            add(y, zb, i, everything)

    lower = z < nz - 1 - z
    for t in range(1, nz):
        relay_own(t)
        relay_other(t - 1)
        take_side(t - 1)
        if t == 1:

            @pl.when(jnp.logical_not(inner))
            def _():
                loop(1, lambda p: both_ways(y, z, 1, p))

        elif t - 1 <= (nz - 1) // 2:
            pl.when((low == t - 1) & lower)(lambda: finish_way(True, t - 1))
            pl.when((low == t - 1) & jnp.logical_not(lower))(lambda: finish_way(False, t - 1))
        if t > 1:
            add_others(t - 2)
    if nz > 1:
        add_others(nz - 2)
    pl.when(jnp.logical_not(inner))(lambda: take_side(nz - 1))
    relay_other(nz - 1)

    @pl.when(inner)
    def _():
        pl.when(lower)(lambda: finish_way(False, nz - 1))
        pl.when(jnp.logical_not(lower))(lambda: finish_way(True, nz - 1))
        take_side(nz - 1)

    add_others(nz - 1)
    for j in range(1, nx):
        swap((x + j) % nx, 0)

    add_last_rows(0)
    add_own(0)
    for k in range(1, nz):
        if k < nz - 1:
            take_last(k)
        add_last_rows(k)
    def send_out(to):
        return pltpu.make_async_remote_copy(
            src_ref=attn.at[pl.ds(pl.multiple_of(to * tok, tok), tok)],
            dst_ref=out_ref.at[:, pl.ds(pl.multiple_of(s * head, head), head)],
            send_sem=osend, recv_sem=orecv,
            device_id={"sp": to}, device_id_type=MESH,
        )

    scale = head ** (-0.5) * log2e

    def attend(r, i, extent):
        at = pl.multiple_of((r * nx + i) * tok, tok)
        scores = lax.dot_general(
            qkv[pl.ds(at, tok), :head], qkv[:extent, head : 2 * head],
            (((1,), (1,)), ((), ())), preferred_element_type=jnp.float32,
        )
        offset = bias[pl.ds(at, tok), :extent] if kept else bias_of(at, tok, extent)
        scores = scores * scale + offset
        top = jnp.max(scores, axis=1, keepdims=True)
        weights = jnp.exp2(scores - top)
        total = jnp.sum(weights, axis=1, keepdims=True)
        summed = jnp.dot(
            weights.astype(jnp.bfloat16), qkv[:extent, 2 * head :],
            preferred_element_type=jnp.float32,
        )
        attn[pl.ds(at, tok), :] = (summed / total).astype(jnp.bfloat16)

    def attend_beside(r):
        def step(j):
            i = (x + j) % nx
            attend(r, i, (r + 1) * group)
            send_out(r * nx + i).start()

        if nx > 2:
            lax.fori_loop(1, nx, lambda j, carry: (step(j), carry)[1], 0)
        else:
            for j in range(1, nx):
                step(j)

    def attend_far(r):
        attend_beside(r)
        attend(r, x, (r + 1) * group)
        send_out(r * nx + x).start()

    def attend_before(r):
        if nx > 2:
            attend_far(r)
            return
        for i in range(nx):
            attend(r, i, (r * nx + i + 1) * tok)
            send_out(r * nx + i).start()

    def swapped():
        for k in range(1, ny):
            other = (y + k) % ny
            taken = qkv.at[pl.ds(pl.multiple_of(other * group, group), group)]
            pltpu.make_async_remote_copy(
                src_ref=taken, dst_ref=taken, send_sem=qsend.at[k - 1],
                recv_sem=qrecv.at[k - 1], device_id=aside(k), device_id_type=MESH,
            ).wait_recv()

    for j in range(1, nx):
        swap((x + j) % nx, 1)
    if nz > 1:
        take_last(nz - 1)
    for k in range(1, nz - 1):
        add_own(k)

    @pl.when(y > 0)
    def _():
        swapped()
        for r in range(ny - 1):
            pl.when(r < y)(lambda r=r: attend_before(r))

    if nz > 1:
        add_own(nz - 1)
    for i in range(nx):
        for g in range(2):
            qkv[own_rows(i, g), :] = acc[y, i, parts[g], :].astype(jnp.bfloat16)

    @pl.when(y == 0)
    def _():
        attend_beside(0)
        swapped()

    for r in range(1, ny):
        pl.when(r > y)(lambda r=r: attend_far(r))
    for r in range(1, ny):
        pl.when(y == r)(lambda r=r: attend_beside(r))
    for r in range(ny):
        pl.when(y == r)(lambda r=r: attend(r, x, (r + 1) * group))
    out_ref[:, pl.ds(pl.multiple_of(s * head, head), head)] = attn[
        pl.ds(pl.multiple_of(s * tok, tok), tok), :
    ]

    for j in range(1, nx):
        pltpu.make_async_remote_copy(
            src_ref=tok_hbm, dst_ref=xbuf.at[x], send_sem=xsend.at[j - 1],
            recv_sem=xrecv.at[j - 1, 0, 0],
            device_id={"sp": y * nx + (x + j) % nx}, device_id_type=MESH,
        ).wait_send()
    for zb in range(nz):
        upward = (z < nz - 1) & (zb <= z)
        downward = (z > 0) & (zb >= z)
        for h, part in [(y, whole)] + [(h, early_rows) for h in others]:
            pl.when(upward)(lambda: up(h, zb, part, 0).wait_send())
            pl.when(downward)(lambda: down(h, zb, part, 0).wait_send())
    if cores > 1:
        sent = wbuf.at[:, :, c]
        pltpu.make_async_remote_copy(
            src_ref=sent, dst_ref=sent, send_sem=psem, recv_sem=precv.at[0, 0],
            device_id=beside, device_id_type=MESH,
        ).wait_send()
    for k in range(1, ny):
        copy_block(
            y, z, c, early_rows, sideq.at[k - 1], farrecv.at[ny - k - 1, z, 0], aside(k)
        ).wait_send()
        sent = wbuf.at[y, :, c, late_rows]
        pltpu.make_async_remote_copy(
            src_ref=sent, dst_ref=sent, send_sem=sidesem.at[k - 1],
            recv_sem=farrecv.at[ny - k - 1, z, 0], device_id=aside(k), device_id_type=MESH,
        ).wait_send()
        pltpu.make_async_remote_copy(
            src_ref=qout.at[k - 1], dst_ref=qout.at[k - 1], send_sem=qsend.at[k - 1],
            recv_sem=qrecv.at[k - 1], device_id=aside(k), device_id_type=MESH,
        ).wait_send()
    rest = attn.at[pl.ds(0, length - tok)]
    ends = pltpu.make_async_remote_copy(
        src_ref=rest, dst_ref=rest, send_sem=osend, recv_sem=orecv,
        device_id={"sp": (s + 1) % (nx * ny)}, device_id_type=MESH,
    )
    ends.wait_recv()
    ends.wait_send()


def body(sp, dp, tokens, query_weight, key_weight, value_weight, cum_gate):
    nx = max(n for n in range(1, math.isqrt(sp) + 1) if sp % n == 0)
    ny = sp // nx
    cores = 2 if dp % 2 == 0 else 1
    nz = dp // cores
    tok, depth = tokens.shape[1:]
    rows, head = query_weight.shape
    length = sp * tok
    split = tok * 5 // 6 // 16 * 16
    early = rows * 5 // 16
    kept = length * length * 4 <= 8 * 1024 * 1024
    cuts = max(rows // 256, 1), 1
    dma = pltpu.SemaphoreType.DMA
    hbm = pl.BlockSpec(memory_space=pltpu.HBM)
    vmem = pl.BlockSpec(memory_space=pltpu.VMEM)
    out = pl.pallas_call(
        functools.partial(kernel, nx, ny, nz, cores, split, early, cuts, kept),
        out_shape=pltpu.VMEM((tok, sp * head), jnp.bfloat16),
        in_specs=[hbm] * 5,
        out_specs=vmem,
        scratch_shapes=[
            pltpu.VMEM((nx, tok, depth), jnp.bfloat16),
            pltpu.VMEM((ny, nz, cores, rows, 3 * head), jnp.bfloat16),
            pltpu.VMEM((ny, nx, tok, 3 * head), jnp.float32),
            pltpu.VMEM((length, 3 * head), jnp.bfloat16),
            pltpu.VMEM((ny - 1, nx, tok, 3 * head), jnp.bfloat16),
            pltpu.VMEM((1, length), jnp.float32),
            pltpu.VMEM((length, 128), jnp.float32),
            pltpu.VMEM((length, head), jnp.bfloat16),
            pltpu.VMEM((length, length) if kept else (8, 128), jnp.float32),
            dma,
            dma,
            dma,
            dma((nx - 1,)),
            dma((nx - 1, nz, 2)),
            dma((max(nz - 1, 1), sum(cuts))),
            dma((ny - 1, nz, cuts[1] + 1)),
            dma((ny, nz)),
            dma((ny, nz + 1)),
            dma((ny - 1,)),
            dma((ny - 1,)),
            dma,
            dma((ny - 1,)),
            dma((ny - 1,)),
            dma,
            dma,
        ],
        compiler_params=pltpu.CompilerParams(
            collective_id=0, has_side_effects=True, vmem_limit_bytes=60 * 1024 * 1024
        ),
    )(tokens[0], query_weight, key_weight, value_weight, cum_gate[0])
    return out[None]


def solution(mesh):
    in_specs = (
        P("dp", "sp", None),
        P("dp", "sp"),
        P("dp", "sp"),
        P("dp", "sp"),
        P("dp", "sp", None),
    )
    out_specs = P("dp", "sp", None)
    return jax.shard_map(
        functools.partial(body, mesh.shape["sp"], mesh.shape["dp"]),
        mesh=mesh, in_specs=in_specs, out_specs=out_specs, check_vma=False,
    )
```

profile of v0, /device:TPU:0, one launch (start us, length us, event | category | flops | bytes accessed | tf_op | source)
XLA Modules:
  0.0 47.1 jit_solution(10171301613303215345)
XLA Ops:
  0.0 46.4 %shard_map.55 = bf16[192,512]{1,0:T(8,128)(2,1)S(1)} custom-call(bf16[192,4096]{1,0:T(8,128)(2,1)} %bitcast.4, bf16[512,128]{1,0:T(8,128)(2,1)} %wq_hbm.1, bf16[512,128]{1,0:T(8,128)(2,1)} %wk_hbm.1, bf16[512,128]{1,0:T(8,128)(2,1)} %wv_hbm.1, f32[1,768]{1,0:T(1,128)} %bitcast.5), custom_call_target="tpu_custom_call" | custom-call | tf_op jit(solution)/shard_map/pallas_call | solution.py:512
  46.5 0.7 %copy.7 = bf16[1,192,512]{2,1,0:T(8,128)(2,1)} copy(bf16[1,192,512]{2,1,0:T(8,128)(2,1)S(1)} %bitcast.3) | data formatting | bytes 393216
where the time goes:
time: 47.3 us; the launch traced here: 47.1 us
  Pallas kernels  46.4 us (98%)
  local copies, waits for them, and re-layouts  0.68 us (1%)
    pallas_call x1, Pallas kernels, body(): pl.pallas_call(functools.partial(kernel, nx, ny, nz, cores, split, early,...  46.4 us

commit v1 on v0

--- a/solution.py
+++ b/solution.py
@@ -502,10 +502,10 @@
     tok, depth = tokens.shape[1:]
     rows, head = query_weight.shape
     length = sp * tok
-    split = tok * 5 // 6 // 16 * 16
-    early = rows * 5 // 16
+    split = tok * 11 // 12 // 16 * 16
+    early = rows * 11 // 32
     kept = length * length * 4 <= 8 * 1024 * 1024
-    cuts = max(rows // 256, 1), 1
+    cuts = 3, 1
     dma = pltpu.SemaphoreType.DMA
     hbm = pl.BlockSpec(memory_space=pltpu.HBM)
     vmem = pl.BlockSpec(memory_space=pltpu.VMEM)

time: 47.3 us -> 47.3 us (level)
  no operation moved by 1% of the time
where the time goes in v1:
time: 47.3 us; the launch traced here: 47.2 us
  Pallas kernels  46.5 us (98%)
  local copies, waits for them, and re-layouts  0.68 us (1%)
    pallas_call x1, Pallas kernels, body(): pl.pallas_call(functools.partial(kernel, nx, ny, nz, cores, split, early,...  46.5 us

profile of v1, /device:TPU:0, one launch (start us, length us, event | category | flops | bytes accessed | tf_op | source)
XLA Modules:
  0.0 47.2 jit_solution(5571331015631542826)
XLA Ops:
  0.0 46.5 %shard_map.55 = bf16[192,512]{1,0:T(8,128)(2,1)S(1)} custom-call(bf16[192,4096]{1,0:T(8,128)(2,1)} %bitcast.4, bf16[512,128]{1,0:T(8,128)(2,1)} %wq_hbm.1, bf16[512,128]{1,0:T(8,128)(2,1)} %wk_hbm.1, bf16[512,128]{1,0:T(8,128)(2,1)} %wv_hbm.1, f32[1,768]{1,0:T(1,128)} %bitcast.5), custom_call_target="tpu_custom_call" | custom-call | tf_op jit(solution)/shard_map/pallas_call | solution.py:512
  46.5 0.7 %copy.7 = bf16[1,192,512]{2,1,0:T(8,128)(2,1)} copy(bf16[1,192,512]{2,1,0:T(8,128)(2,1)S(1)} %bitcast.3) | data formatting | bytes 393216
